TPU v7x, 32 devices: a whole 2x2x4 slice. The times are simulated.
32 devices in a mesh: fs: 8 (over z, core), tp: 4 (over y, x).
Axes of the slice: x: 2, y: 2, z: 4, core: 2. Of those that a mesh axis runs over, the one named last changes fastest.
Arguments:
- saved_input: bfloat16 [6144, 2048], P('fs'), may hold values from -6 to 6
- query_cot: bfloat16 [6144, 2048], P('fs', 'tp'), may hold values from -120 to 120
- head_out: bfloat16 [6144, 2048], P('fs', 'tp'), may hold values from -120 to 120
- output_cot: bfloat16 [6144, 2048], P('fs'), may hold values from -6 to 6
- basis_q: bfloat16 [2048, 128], replicated, may hold values from -0.125 to 0.125
- basis_o: bfloat16 [2048, 128], replicated, may hold values from -0.125 to 0.125
- weight_q: float32 [2048, 2048], P('fs', 'tp'), may hold values from -0.125 to 0.125
- weight_o: float32 [2048, 2048], P('tp', 'fs'), may hold values from -0.125 to 0.125
- first_q: float32 [128, 2048], P(None, 'tp'), may hold values from -2 to 2
- second_q: float32 [128, 2048], P(None, 'tp'), may hold values from 0.01 to 1
- first_o: float32 [2048, 128], P('tp'), may hold values from -2 to 2
- second_o: float32 [2048, 128], P('tp'), may hold values from 0.01 to 1
Outputs:
- step_q: float32 [2048, 2048], P('fs', 'tp')
- step_o: float32 [2048, 2048], P('tp', 'fs')
- new_weight_q: float32 [2048, 2048], P('fs', 'tp')
- new_weight_o: float32 [2048, 2048], P('tp', 'fs')
- copy_q: bfloat16 [2048, 2048], P(None, 'tp')
- copy_o: bfloat16 [2048, 2048], P('tp')
- moment_q: float32 [128, 2048], P(None, 'tp')
- square_q: float32 [128, 2048], P(None, 'tp')
- moment_o: float32 [2048, 128], P('tp')
- square_o: float32 [2048, 128], P('tp')
All inputs are finite; a program needn't handle non-finite values.
Results may differ from a plain program's by a relative error of at most 0.0035.
Values may be sent and summed in bfloat16 or wider, within the bound.
A program may use at most 64 MiB of HBM per device.

v0:
```python
import jax
import jax.numpy as jnp
from jax import lax
from jax.sharding import PartitionSpec as P

HEADS = 16
HEAD = 128
RANK = 128
BETA_FIRST = 0.9
BETA_SECOND = 0.95
ADAM_EPS = 1e-08
NORM_EPS = 1e-06
CLIP_RMS = 1.0
LEARN_RATE = 0.01


def split_product(factor_part, data_part):
    upper = factor_part.astype(jnp.bfloat16)
    lower = (factor_part - upper.astype(jnp.float32)).astype(jnp.bfloat16)
    first = jnp.dot(upper, data_part, preferred_element_type=jnp.float32)
    return first + jnp.dot(lower, data_part, preferred_element_type=jnp.float32)


def shards(
    saved_input,
    query_cot,
    head_out,
    output_cot,
    basis_q,
    basis_o,
    weight_q,
    weight_o,
    first_q,
    second_q,
    first_o,
    second_o,
):
    highest = lax.Precision.HIGHEST
    row_count = weight_q.shape[0]
    offset = lax.axis_index("fs") * row_count
    rows_q = lax.dynamic_slice_in_dim(basis_q, offset, row_count, 0).astype(jnp.float32)
    rows_o = lax.dynamic_slice_in_dim(basis_o, offset, row_count, 0).astype(jnp.float32)
    input_low = jnp.dot(saved_input, basis_q, preferred_element_type=jnp.float32)
    partial_q = split_product(input_low.T, query_cot)
    cot_low = jnp.dot(output_cot, basis_o, preferred_element_type=jnp.float32)
    partial_o = split_product(cot_low.T, head_out).T
    low_q, low_o = lax.psum((partial_q, partial_o), "fs")
    sum_q, sum_o = lax.psum((jnp.sum(low_q * low_q), jnp.sum(low_o * low_o)), "tp")
    rms_value = jnp.sqrt((sum_q + sum_o) / (2 * RANK * HEADS * HEAD) + NORM_EPS)
    factor = jnp.minimum(1.0, CLIP_RMS / rms_value)
    moment_q = BETA_FIRST * first_q + (1.0 - BETA_FIRST) * factor * low_q
    square_q = BETA_SECOND * second_q + (1.0 - BETA_SECOND) * (factor * low_q) ** 2
    moment_o = BETA_FIRST * first_o + (1.0 - BETA_FIRST) * factor * low_o
    square_o = BETA_SECOND * second_o + (1.0 - BETA_SECOND) * (factor * low_o) ** 2
    dir_q = moment_q / (jnp.sqrt(square_q) + ADAM_EPS)
    dir_o = moment_o / (jnp.sqrt(square_o) + ADAM_EPS)
    step_q = jnp.dot(rows_q, dir_q, precision=highest)
    step_o = jnp.dot(dir_o, rows_o.T, precision=highest)
    new_weight_q = weight_q - LEARN_RATE * step_q
    new_weight_o = weight_o - LEARN_RATE * step_o
    copy_q, copy_o = (
        lax.all_gather(new_weight_q.astype(jnp.bfloat16), "fs", axis=0, tiled=True),
        lax.all_gather(new_weight_o.astype(jnp.bfloat16), "fs", axis=1, tiled=True),
    )
    return (
        step_q,
        step_o,
        new_weight_q,
        new_weight_o,
        copy_q,
        copy_o,
        moment_q,
        square_q,
        moment_o,
        square_o,
    )


def solution(mesh):
    return jax.shard_map(
        shards,
        mesh=mesh,
        in_specs=(
            P("fs", None),
            P("fs", "tp"),
            P("fs", "tp"),
            P("fs", None),
            P(),
            P(),
            P("fs", "tp"),
            P("tp", "fs"),
            P(None, "tp"),
            P(None, "tp"),
            P("tp", None),
            P("tp", None),
        ),
        out_specs=(
            P("fs", "tp"),
            P("tp", "fs"),
            P("fs", "tp"),
            P("tp", "fs"),
            P(None, "tp"),
            P("tp", None),
            P(None, "tp"),
            P(None, "tp"),
            P("tp", None),
            P("tp", None),
        ),
        check_vma=False,
    )
```

profile of v0, /device:TPU:0, one launch (start us, length us, event | category | flops | bytes accessed | tf_op | source)
XLA Modules:
  0.0 164.3 jit_solution(583530073985837648)
XLA Ops:
  7.2 0.0 copy-start
  7.2 0.0 all-reduce.3.cloned.1.call-start
  7.2 1.8 %copy-done = bf16[768,2048]{1,0:T(8,128)(2,1)S(1)} copy-done((bf16[768,2048]{1,0:T(8,128)(2,1)S(1)}, bf16[768,2048]{1,0:T(8,128)(2,1)}, u32[]{:S(2)}) %copy-start) | copy-done | bytes 3145752
  9.1 0.0 copy-start.2
  9.1 0.0 copy-start.1
  9.1 0.0 copy-start.8
  9.1 2.4 %fusion.25 = f32[128,768]{1,0:T(8,128)S(1)} fusion(bf16[2048,128]{1,0:T(8,128)(2,1)} %param.16, bf16[768,2048]{1,0:T(8,128)(2,1)S(1)} %copy-done), kind=kOutput, calls=%fused_computation.37 | convolution fusion | flops 402653184 | bytes 4063232 | tf_op jit(solution)/shard_map/dot_general | solution.py:43
  11.4 0.0 copy-done.2
  11.5 0.3 fusion.15
  11.7 0.0 copy-start.3
  11.7 1.0 convolution_add_fusion.1
  12.7 0.0 copy-done.1
  12.7 0.0 copy-done.8
  12.7 0.0 copy-start.9
  12.7 1.2 fusion.26
  13.9 0.0 copy-done.3
  13.9 0.3 fusion.12
  14.2 1.0 fusion
  15.2 0.0 all-reduce.3.cloned.1.call-update
  15.2 0.0 all-gather.5.cloned.1.call-start
  15.2 0.0 copy-done.9
  15.2 0.8 copy.22
  16.1 1.8 %copy.23 = f32[512,128]{0,1:T(8,128)} copy(f32[512,128]{1,0:T(8,128)} %param.23) | data formatting | bytes 524288 | tf_op args[11]
  17.9 56.8 %all-reduce.3.cloned.1.call-done = (f32[128,512]{1,0:T(8,128)}, f32[512,128]{0,1:T(8,128)}) async-done(((f32[128,512]{1,0:T(8,128)}, f32[512,128]{0,1:T(8,128)}), (f32[128,512]{1,0:T(8,128)}, f32[512,128]{0,1:T(8,128)})) %all-reduce.3.cloned.1.call-update) | async-done | bytes 524304 | tf_op jit(solution)/shard_map/psum | solution.py:47
  74.7 1.6 multiply_reduce_fusion
  76.3 1.6 multiply_reduce_fusion.1
  79.2 10.3 %psum.32 = f32[]{:T(128)} all-reduce(f32[]{:T(128)S(6)} %add.56), channel_id=1, replica_groups=mesh['fs'=8,'tp'=4] {'tp'}, use_global_device_ids=true, to_apply=%region_2.0 | all-reduce | flops 1 | bytes 8 | tf_op jit(solution)/shard_map/psum | solution.py:48
  90.3 1.2 multiply_add_fusion
  91.5 0.0 copy-start.4
  91.5 0.7 copy-done.4
  92.2 2.6 %fusion.23 = (bf16[512,256]{1,0:T(8,128)(2,1)}, f32[512,256]{1,0:T(8,128)}, f32[512,256]{1,0:T(8,128)}) fusion(f32[512,256]{1,0:T(8,128)} %param.19, bf16[2048,128]{1,0:T(8,128)(2,1)} %param.17, s32[]{:T(128)S(6)} %select_n.4, f32[512,128]{0,1:T(8,128)S(1)} %get-tuple-element.27, f32[512,128]{0,1:T(8,128)S(1)} %get-tuple-element.26), kind=kOutput, calls=%fused_computation.35 | convolution fusion | flops 201850880 | bytes 2424836 | tf_op jit(solution)/shard_map/dot_general | solution.py:58
  94.8 0.0 all-gather.5.cloned.1.call-update
  94.8 0.0 all-gather.3.cloned.1.call-start
  94.9 1.2 multiply_add_fusion.2
  96.1 0.0 copy-start.6
  96.1 0.0 copy-start.7
  96.1 0.7 copy-done.6
  96.8 2.6 %fusion.24 = (bf16[256,512]{1,0:T(8,128)(2,1)}, f32[256,512]{1,0:T(8,128)}, f32[256,512]{1,0:T(8,128)}) fusion(f32[256,512]{1,0:T(8,128)} %param.18, f32[128,512]{1,0:T(8,128)S(1)} %get-tuple-element.48, f32[128,512]{1,0:T(8,128)S(1)} %get-tuple-element.49, bf16[2048,128]{1,0:T(8,128)(2,1)} %param.16, s32[]{:T(128)S(6)} %select_n.4), kind=kOutput, calls=%fused_computation.36 | convolution fusion | flops 201850880 | bytes 2424836 | tf_op jit(solution)/shard_map/dot_general | solution.py:57
  99.4 0.0 copy-done.7
  99.4 0.0 all-gather.3.cloned.1.call-update
  99.4 1.8 %copy.25 = f32[512,128]{1,0:T(8,128)} copy(f32[512,128]{0,1:T(8,128)} %copy-done.4) | data formatting | bytes 524288
  101.2 0.8 copy.24
  102.1 20.8 %all-gather.5.cloned.1.call-done = bf16[512,2048]{1,0:T(8,128)(2,1)} async-done(((bf16[512,256]{1,0:T(8,128)(2,1)}), bf16[512,2048]{1,0:T(8,128)(2,1)}) %all-gather.5.cloned.1.call-update) | async-done | bytes 2097168 | tf_op jit(solution)/shard_map/all_gather | solution.py:63
  122.8 30.4 %all-gather.3.cloned.1.call-done = bf16[2048,512]{1,0:T(8,128)(2,1)} async-done(((bf16[256,512]{1,0:T(8,128)(2,1)}), bf16[2048,512]{1,0:T(8,128)(2,1)}) %all-gather.3.cloned.1.call-update) | async-done | bytes 2097168 | tf_op jit(solution)/shard_map/all_gather | solution.py:62
  153.2 0.0 copy-start.5
  153.2 3.2 %copy.30 = bf16[2048,512]{1,0:T(8,128)(2,1)} copy(bf16[2048,512]{1,0:T(8,128)(2,1)} %all-gather.3.cloned.1.call-done) | data formatting | bytes 4194304
  156.4 0.0 copy-done.5
  156.4 1.3 copy.31
Async XLA Ops:
  7.2 1.9 %copy-start = (bf16[768,2048]{1,0:T(8,128)(2,1)S(1)}, bf16[768,2048]{1,0:T(8,128)(2,1)}, u32[]{:S(2)}) copy-start(bf16[768,2048]{1,0:T(8,128)(2,1)} %param.12) | copy-start | bytes 9437188
  7.2 67.5 %all-reduce.3.cloned.1.call-start = ((), (), s32[]{:S(2)}) async-start(), calls=%async_computation.2 | async-start | bytes 1048576 | tf_op jit(solution)/shard_map/psum | solution.py:47
  9.1 2.4 %copy-start.2 = (bf16[768,512]{1,0:T(8,128)(2,1)S(1)}, bf16[768,512]{1,0:T(8,128)(2,1)}, u32[]{:S(2)}) copy-start(bf16[768,512]{1,0:T(8,128)(2,1)} %param.13) | copy-start | bytes 2359300
  9.1 3.6 %copy-start.1 = (bf16[768,2048]{1,0:T(8,128)(2,1)S(1)}, bf16[768,2048]{1,0:T(8,128)(2,1)}, u32[]{:S(2)}) copy-start(bf16[768,2048]{1,0:T(8,128)(2,1)} %param.15) | copy-start | bytes 9437188
  9.1 3.6 %copy-start.8 = (bf16[2048,128]{1,0:T(8,128)(2,1)S(1)}, bf16[2048,128]{1,0:T(8,128)(2,1)}, u32[]{:S(2)}) copy-start(bf16[2048,128]{1,0:T(8,128)(2,1)} %param.17) | copy-start | bytes 1572868
  11.7 2.2 %copy-start.3 = (bf16[768,512]{1,0:T(8,128)(2,1)S(1)}, bf16[768,512]{1,0:T(8,128)(2,1)}, u32[]{:S(2)}) copy-start(bf16[768,512]{1,0:T(8,128)(2,1)} %param.14) | copy-start | bytes 2359300
  12.7 2.5 %copy-start.9 = (f32[512,128]{1,0:T(8,128)S(1)}, f32[512,128]{1,0:T(8,128)}, u32[]{:S(2)}) copy-start(f32[512,128]{1,0:T(8,128)} %param.22) | copy-start | bytes 786436
  15.2 107.7 %all-gather.5.cloned.1.call-start = ((), (), s32[]{:S(2)}) async-start(), calls=%async_computation.1 | async-start | bytes 2359296 | tf_op jit(solution)/shard_map/all_gather | solution.py:63
  91.5 0.7 copy-start.4
  94.8 58.4 %all-gather.3.cloned.1.call-start = ((), (), s32[]{:S(2)}) async-start(), calls=%async_computation | async-start | bytes 2359296 | tf_op jit(solution)/shard_map/all_gather | solution.py:62
  96.1 0.7 copy-start.6
  96.1 3.3 %copy-start.7 = (f32[128,512]{1,0:T(8,128)}, f32[128,512]{1,0:T(8,128)S(1)}, u32[]{:S(2)}) copy-start(f32[128,512]{1,0:T(8,128)S(1)} %get-tuple-element.48) | copy-start | bytes 786436
  153.2 3.2 %copy-start.5 = (bf16[512,2048]{1,0:T(8,128)(2,1)S(1)}, bf16[512,2048]{1,0:T(8,128)(2,1)}, u32[]{:S(2)}) copy-start(bf16[512,2048]{1,0:T(8,128)(2,1)} %all-gather.5.cloned.1.call-done) | copy-start | bytes 6291460
Sparse Core Ops, SparseCore 0:
  15.3 59.3 all-reduce.2
  94.9 27.8 all-gather.4
  125.0 28.1 all-gather.2
where the time goes:
time: 165 us; the launch traced here: 164 us
  waiting for transfers between devices  108 us (65%)
  between operations  15.9 us (10%)
  local copies, waits for them, and re-layouts  13 us (8%)
  matrix products  11.2 us (7%)
  blocking collectives  10.3 us (6%)
  other arithmetic  5.64 us (3%)
    psum x1, waiting for transfers between devices, shards(): low_q, low_o = lax.psum((partial_q, partial_o), 'fs')  56.8 us
    all_gather x1, waiting for transfers between devices, shards(): lax.all_gather(new_weight_q.astype(jnp.bfloat16), 'fs', axis=0, tiled=True)  30.4 us
    all_gather x1, waiting for transfers between devices, shards(): lax.all_gather(new_weight_o.astype(jnp.bfloat16), 'fs', axis=1, tiled=True)  20.8 us
    unnamed x26, local copies, waits for them, and re-layouts  13 us
    psum x1, blocking collectives, shards(): lax.psum((jnp.sum(low_q * low_q), jnp.sum(low_o * low_o)), 'tp')  10.3 us
  transfers between devices with their start and end apart: 3, of which 3 were waited for; matrix products, arithmetic and copies ran while one was open for 6% of the time, Pallas kernels for 0%

commit v1 on v0

--- a/solution.py
+++ b/solution.py
@@ -12,6 +12,11 @@
 NORM_EPS = 1e-06
 CLIP_RMS = 1.0
 LEARN_RATE = 0.01
+
+
+def pair_yards(vec, axis_id):
+    z1 = lax.all_gather(vec, axis_id)
+    return jnp.concatenate(z1, axis=1)
 
 
 def split_product(factor_part, data_part):
@@ -60,7 +65,7 @@
     new_weight_o = weight_o - LEARN_RATE * step_o
     copy_q, copy_o = (
         lax.all_gather(new_weight_q.astype(jnp.bfloat16), "fs", axis=0, tiled=True),
-        lax.all_gather(new_weight_o.astype(jnp.bfloat16), "fs", axis=1, tiled=True),
+        pair_yards(new_weight_o.astype(jnp.bfloat16), "fs"),
     )
     return (
         step_q,

time: 165 us -> 162 us (0.982)
  waiting for transfers between devices: 108 us -> 104 us
  local copies, waits for them, and re-layouts: 13 us -> 14.7 us
    reshape x0 -> x1, local copies, waits for them, and re-layouts: none -> 3.19 us  [pair_yards(): return jnp.concatenate(z1, axis=1)]
    all_gather x1, waiting for transfers between devices: 30.4 us -> 27.6 us  [shards(): lax.all_gather(new_weight_q.astype(jnp.bfloat16), 'fs', axis=0, tiled=True)]
    unnamed x26 -> x23, local copies, waits for them, and re-layouts: 13 us -> 11.5 us
  transfers between devices with their start and end apart: 3 -> 3, of which waited for: 3 -> 3; matrix products, arithmetic and copies ran while one was open for 6% -> 8% of each run, Pallas kernels for 0% -> 0%
where the time goes in v1:
time: 162 us
  waiting for transfers between devices  104 us (64%)
  between operations  15.9 us (10%)
  local copies, waits for them, and re-layouts  14.7 us (9%)
  matrix products  11.2 us (7%)
  blocking collectives  10.3 us (6%)
  other arithmetic  5.64 us (3%)
    psum x1, waiting for transfers between devices, shards(): low_q, low_o = lax.psum((partial_q, partial_o), 'fs')  56.8 us
    all_gather x1, waiting for transfers between devices, shards(): lax.all_gather(new_weight_q.astype(jnp.bfloat16), 'fs', axis=0, tiled=True)  27.6 us
    all_gather x1, waiting for transfers between devices, pair_yards(): z1 = lax.all_gather(vec, axis_id)  19.3 us
    unnamed x23, local copies, waits for them, and re-layouts  11.5 us
    psum x1, blocking collectives, shards(): lax.psum((jnp.sum(low_q * low_q), jnp.sum(low_o * low_o)), 'tp')  10.3 us
  transfers between devices with their start and end apart: 3, of which 3 were waited for; matrix products, arithmetic and copies ran while one was open for 8% of the time, Pallas kernels for 0%

profile of v1, /device:TPU:0, one launch (start us, length us, event | category | flops | bytes accessed | tf_op | source)
XLA Modules:
  0.0 161.7 jit_solution(15809549713658101379)
XLA Ops:
  7.2 0.0 copy-start
  7.2 0.0 all-reduce.3.cloned.1.call-start
  7.2 1.8 %copy-done = bf16[768,2048]{1,0:T(8,128)(2,1)S(1)} copy-done((bf16[768,2048]{1,0:T(8,128)(2,1)S(1)}, bf16[768,2048]{1,0:T(8,128)(2,1)}, u32[]{:S(2)}) %copy-start) | copy-done | bytes 3145752
  9.1 0.0 copy-start.2
  9.1 0.0 copy-start.1
  9.1 0.0 copy-start.7
  9.1 2.4 %fusion.25 = f32[128,768]{1,0:T(8,128)S(1)} fusion(bf16[2048,128]{1,0:T(8,128)(2,1)} %param.16, bf16[768,2048]{1,0:T(8,128)(2,1)S(1)} %copy-done), kind=kOutput, calls=%fused_computation.37 | convolution fusion | flops 402653184 | bytes 4063232 | tf_op jit(solution)/shard_map/dot_general | solution.py:48
  11.4 0.0 copy-done.2
  11.5 0.3 fusion.15
  11.7 0.0 copy-start.3
  11.7 1.0 convolution_add_fusion.1
  12.7 0.0 copy-done.1
  12.7 0.0 copy-done.7
  12.7 0.0 copy-start.8
  12.7 1.2 fusion.26
  13.9 0.0 copy-done.3
  13.9 0.3 fusion.12
  14.2 1.0 fusion
  15.2 0.0 all-reduce.3.cloned.1.call-update
  15.2 0.0 all-gather.6.cloned.1.call-start
  15.2 0.0 copy-done.8
  15.2 0.8 copy.22
  16.1 1.8 %copy.23 = f32[512,128]{0,1:T(8,128)} copy(f32[512,128]{1,0:T(8,128)} %param.23) | data formatting | bytes 524288 | tf_op args[11]
  17.9 56.8 %all-reduce.3.cloned.1.call-done = (f32[128,512]{1,0:T(8,128)}, f32[512,128]{0,1:T(8,128)}) async-done(((f32[128,512]{1,0:T(8,128)}, f32[512,128]{0,1:T(8,128)}), (f32[128,512]{1,0:T(8,128)}, f32[512,128]{0,1:T(8,128)})) %all-reduce.3.cloned.1.call-update) | async-done | bytes 524304 | tf_op jit(solution)/shard_map/psum | solution.py:52
  74.7 1.6 %multiply_reduce_fusion = f32[]{:T(128)} fusion(f32[512,128]{0,1:T(8,128)} %get-tuple-element.21), kind=kLoop, calls=%fused_computation.19 | loop fusion | flops 131071 | bytes 262148 | tf_op jit(solution)/shard_map/reduce_sum | solution.py:53
  76.3 1.6 %multiply_reduce_fusion.1 = f32[]{:T(128)} fusion(f32[128,512]{1,0:T(8,128)} %get-tuple-element.20), kind=kLoop, calls=%fused_computation.20 | loop fusion | flops 131071 | bytes 262148 | tf_op jit(solution)/shard_map/reduce_sum | solution.py:53
  79.2 10.3 %psum.32 = f32[]{:T(128)} all-reduce(f32[]{:T(128)S(6)} %add.56), channel_id=1, replica_groups=mesh['fs'=8,'tp'=4] {'tp'}, use_global_device_ids=true, to_apply=%region_2.0 | all-reduce | flops 1 | bytes 8 | tf_op jit(solution)/shard_map/psum | solution.py:53
  90.3 1.2 multiply_add_fusion
  91.5 0.0 copy-start.4
  91.5 0.7 copy-done.4
  92.2 2.6 %fusion.23 = (bf16[512,256]{1,0:T(8,128)(2,1)}, f32[512,256]{1,0:T(8,128)}, f32[512,256]{1,0:T(8,128)}) fusion(f32[512,256]{1,0:T(8,128)} %param.19, bf16[2048,128]{1,0:T(8,128)(2,1)} %param.17, s32[]{:T(128)S(6)} %select_n.4, f32[512,128]{0,1:T(8,128)S(1)} %get-tuple-element.27, f32[512,128]{0,1:T(8,128)S(1)} %get-tuple-element.26), kind=kOutput, calls=%fused_computation.35 | convolution fusion | flops 201850880 | bytes 2424836 | tf_op jit(solution)/shard_map/dot_general | solution.py:63
  94.8 0.0 all-gather.6.cloned.1.call-update
  94.8 0.0 all-gather.4.cloned.1.call-start
  94.9 1.2 multiply_add_fusion.2
  96.1 0.0 copy-start.5
  96.1 0.0 copy-start.6
  96.1 0.7 copy-done.5
  96.8 2.6 %fusion.24 = (bf16[256,512]{1,0:T(8,128)(2,1)}, f32[256,512]{1,0:T(8,128)}, f32[256,512]{1,0:T(8,128)}) fusion(f32[256,512]{1,0:T(8,128)} %param.18, f32[128,512]{1,0:T(8,128)S(1)} %get-tuple-element.48, f32[128,512]{1,0:T(8,128)S(1)} %get-tuple-element.49, bf16[2048,128]{1,0:T(8,128)(2,1)} %param.16, s32[]{:T(128)S(6)} %select_n.4), kind=kOutput, calls=%fused_computation.36 | convolution fusion | flops 201850880 | bytes 2424836 | tf_op jit(solution)/shard_map/dot_general | solution.py:62
  99.4 0.0 copy-done.6
  99.4 0.0 all-gather.4.cloned.1.call-update
  99.4 1.8 %copy.26 = f32[512,128]{1,0:T(8,128)} copy(f32[512,128]{0,1:T(8,128)} %copy-done.4) | data formatting | bytes 524288
  101.2 0.8 copy.25
  102.1 19.3 %all-gather.6.cloned.1.call-done = bf16[4096,256]{1,0:T(8,128)(2,1)} async-done(((bf16[512,256]{1,0:T(8,128)(2,1)}), bf16[4096,256]{1,0:T(8,128)(2,1)}) %all-gather.6.cloned.1.call-update) | async-done | bytes 2097168 | tf_op jit(solution)/shard_map/all_gather | solution.py:18
  121.4 3.2 %copy.27 = bf16[8,64,8,256]{3,2,0,1:T(8,128)(2,1)} copy(bf16[8,64,8,256]{3,2,1,0:T(8,128)(2,1)} %bitcast.15) | data formatting | bytes 4194304 | tf_op jit(solution)/shard_map/reshape | solution.py:19
  124.6 27.6 %all-gather.4.cloned.1.call-done = bf16[2048,512]{1,0:T(8,128)(2,1)} async-done(((bf16[256,512]{1,0:T(8,128)(2,1)}), bf16[2048,512]{1,0:T(8,128)(2,1)}) %all-gather.4.cloned.1.call-update) | async-done | bytes 2097168 | tf_op jit(solution)/shard_map/all_gather | solution.py:67
  152.1 3.0 %copy.31 = bf16[2048,512]{1,0:T(8,128)(2,1)} copy(bf16[2048,512]{1,0:T(8,128)(2,1)} %all-gather.4.cloned.1.call-done) | data formatting | bytes 4194304
Async XLA Ops:
  7.2 1.9 %copy-start = (bf16[768,2048]{1,0:T(8,128)(2,1)S(1)}, bf16[768,2048]{1,0:T(8,128)(2,1)}, u32[]{:S(2)}) copy-start(bf16[768,2048]{1,0:T(8,128)(2,1)} %param.12) | copy-start | bytes 9437188
  7.2 67.5 %all-reduce.3.cloned.1.call-start = ((), (), s32[]{:S(2)}) async-start(), calls=%async_computation.2 | async-start | bytes 1048576 | tf_op jit(solution)/shard_map/psum | solution.py:52
  9.1 2.4 %copy-start.2 = (bf16[768,512]{1,0:T(8,128)(2,1)S(1)}, bf16[768,512]{1,0:T(8,128)(2,1)}, u32[]{:S(2)}) copy-start(bf16[768,512]{1,0:T(8,128)(2,1)} %param.13) | copy-start | bytes 2359300
  9.1 3.6 %copy-start.1 = (bf16[768,2048]{1,0:T(8,128)(2,1)S(1)}, bf16[768,2048]{1,0:T(8,128)(2,1)}, u32[]{:S(2)}) copy-start(bf16[768,2048]{1,0:T(8,128)(2,1)} %param.15) | copy-start | bytes 9437188
  9.1 3.6 %copy-start.7 = (bf16[2048,128]{1,0:T(8,128)(2,1)S(1)}, bf16[2048,128]{1,0:T(8,128)(2,1)}, u32[]{:S(2)}) copy-start(bf16[2048,128]{1,0:T(8,128)(2,1)} %param.17) | copy-start | bytes 1572868
  11.7 2.2 %copy-start.3 = (bf16[768,512]{1,0:T(8,128)(2,1)S(1)}, bf16[768,512]{1,0:T(8,128)(2,1)}, u32[]{:S(2)}) copy-start(bf16[768,512]{1,0:T(8,128)(2,1)} %param.14) | copy-start | bytes 2359300
  12.7 2.5 %copy-start.8 = (f32[512,128]{1,0:T(8,128)S(1)}, f32[512,128]{1,0:T(8,128)}, u32[]{:S(2)}) copy-start(f32[512,128]{1,0:T(8,128)} %param.22) | copy-start | bytes 786436
  15.2 106.2 %all-gather.6.cloned.1.call-start = ((), (), s32[]{:S(2)}) async-start(), calls=%async_computation.1 | async-start | bytes 2359296 | tf_op jit(solution)/shard_map/all_gather | solution.py:18
  91.5 0.7 copy-start.4
  94.8 57.3 %all-gather.4.cloned.1.call-start = ((), (), s32[]{:S(2)}) async-start(), calls=%async_computation | async-start | bytes 2359296 | tf_op jit(solution)/shard_map/all_gather | solution.py:67
  96.1 0.7 copy-start.5
  96.1 3.3 %copy-start.6 = (f32[128,512]{1,0:T(8,128)}, f32[128,512]{1,0:T(8,128)S(1)}, u32[]{:S(2)}) copy-start(f32[128,512]{1,0:T(8,128)S(1)} %get-tuple-element.48) | copy-start | bytes 786436
Sparse Core Ops, SparseCore 0:
  15.3 59.3 all-reduce.2
  94.9 26.3 all-gather.5
  123.5 28.5 all-gather.3
